TPU v7x, 256 devices: a whole 4x4x8 slice. The times are simulated.
256 devices in a mesh: fs: 32 (over z, y), tp: 8 (over x, core).
Axes of the slice: x: 4, y: 4, z: 8, core: 2. Of those that a mesh axis runs over, the one named last changes fastest.
Arguments:
- layer_input: bfloat16 [65536, 2048], P('fs'), may hold values from -6 to 6
- input_cotangent: bfloat16 [65536, 2048], P('fs', 'tp'), may hold values from -6 to 6
- gate_cotangent: bfloat16 [65536, 2048], P('fs', 'tp'), may hold values from -6 to 6
- input_weight: float32 [2048, 2048], P('fs', 'tp'), may hold values from -0.125 to 0.125
- gate_weight: float32 [2048, 2048], P('fs', 'tp'), may hold values from -0.125 to 0.125
- input_basis: bfloat16 [2048, 256], P('fs'), may hold values from -1.81196113 to 1.81196113
- gate_basis: bfloat16 [2048, 256], P('fs'), may hold values from -1.81196113 to 1.81196113
- input_first: float32 [256, 2048], P('fs', 'tp'), may hold values from -20992 to 20992
- input_second: float32 [256, 2048], P('fs', 'tp'), may hold values from 65536 to 1966080
- gate_first: float32 [256, 2048], P('fs', 'tp'), may hold values from -20992 to 20992
- gate_second: float32 [256, 2048], P('fs', 'tp'), may hold values from 65536 to 1966080
Outputs:
- input_new: float32 [2048, 2048], P('fs', 'tp')
- gate_new: float32 [2048, 2048], P('fs', 'tp')
- input_step: float32 [2048, 2048], P('fs', 'tp')
- gate_step: float32 [2048, 2048], P('fs', 'tp')
- input_first_new: float32 [256, 2048], P('fs', 'tp')
- input_second_new: float32 [256, 2048], P('fs', 'tp')
- gate_first_new: float32 [256, 2048], P('fs', 'tp')
- gate_second_new: float32 [256, 2048], P('fs', 'tp')
- input_copy: bfloat16 [2048, 2048], P(None, 'tp')
- gate_copy: bfloat16 [2048, 2048], P(None, 'tp')
All inputs are finite; a program needn't handle non-finite values.
Results may differ from a plain program's by a relative error of at most 0.0055.
Values may be sent and summed in bfloat16 or wider, within the bound.
A program may use at most 64 MiB of HBM per device.

v0:
```python
import functools

import jax
import jax.numpy as jnp
from jax import lax
from jax.sharding import Mesh
from jax.sharding import PartitionSpec as P

D = 2048
W = 2048
FS = ("fs_0", "fs_1")
FS_TP = ("fs_0", "fs_1", "tp_0", "tp_1")
TP = ("tp_0", "tp_1")


first_decay = 0.8
second_decay = 0.95
learn_rate = 0.01


def in_one_piece(arrays, axis, dim, along):
    widths = [a.shape[along] for a in arrays]
    both = jnp.concatenate(arrays, axis=along)
    filled = lax.all_gather(both, axis, axis=dim, tiled=True)
    return tuple(jnp.split(filled, [sum(widths[:k]) for k in range(1, len(widths))], axis=along))


def cut_along(x, dim, peers):
    before, after = (x.shape[:dim], x.shape[dim + 1 :])
    return jnp.moveaxis(x.reshape(*before, peers, -1, *after), dim, 0)


def sent_and_summed(x, axis, dim):
    blocks = cut_along(x, dim, lax.axis_size(axis))
    arrived = lax.all_to_all(blocks, axis, split_axis=0, concat_axis=0, tiled=True)
    return arrived.astype(jnp.float32).sum(axis=0)


def in_one_piece_2(arrays, axis, dim, along):
    ends, at = ([], 0)
    for a in arrays[:-1]:
        at += a.shape[along]
        ends.append(at)
    both = jnp.concatenate(arrays, axis=along)
    return tuple(jnp.split(sent_and_summed(both, axis, dim), ends, axis=along))


def by_axis(x, axes):
    return functools.reduce(lax.psum, axes, x)


def moments(small, first, second):
    first_new = first_decay * first + (1.0 - first_decay) * small
    second_new = second_decay * second + (1.0 - second_decay) * small * small
    direction = (first_new / (jnp.sqrt(second_new) + 1e-08)).astype(jnp.bfloat16)
    return (first_new, second_new, direction)


def split_product(projected, cotangent):
    upper = projected.astype(jnp.bfloat16)
    lower = (projected - upper.astype(jnp.float32)).astype(jnp.bfloat16)
    dims = (((0,), (0,)), ((), ()))
    return lax.dot_general(
        upper, cotangent, dims, preferred_element_type=jnp.float32
    ) + lax.dot_general(lower, cotangent, dims, preferred_element_type=jnp.float32)


def shards(
    layer_input,
    input_cotangent,
    gate_cotangent,
    input_weight,
    gate_weight,
    input_basis,
    gate_basis,
    input_first,
    input_second,
    gate_first,
    gate_second,
):
    pieces = in_one_piece((input_basis, gate_basis), FS, 0, 1)
    input_proj = jnp.dot(layer_input, pieces[0], preferred_element_type=jnp.float32)
    gate_proj = jnp.dot(layer_input, pieces[1], preferred_element_type=jnp.float32)
    input_small = split_product(input_proj, input_cotangent)
    gate_small = split_product(gate_proj, gate_cotangent)
    input_part, gate_part = in_one_piece_2(
        (input_small.astype(jnp.bfloat16), gate_small.astype(jnp.bfloat16)), FS, 0, 1
    )
    in_first, in_second, in_direction = moments(input_part, input_first, input_second)
    gt_first, gt_second, gt_direction = moments(gate_part, gate_first, gate_second)
    pieces = in_one_piece((in_direction, gt_direction), FS, 0, 1)
    input_update = jnp.dot(input_basis, pieces[0], preferred_element_type=jnp.float32)
    gate_update = jnp.dot(gate_basis, pieces[1], preferred_element_type=jnp.float32)
    input_squares, gate_squares = (
        by_axis(jnp.sum(input_update * input_update), FS_TP),
        by_axis(jnp.sum(gate_update * gate_update), FS_TP),
    )
    input_factor = jnp.minimum(1.0, 1.0 / jnp.sqrt(input_squares / (D * W) + 1e-06))
    gate_factor = jnp.minimum(1.0, 1.0 / jnp.sqrt(gate_squares / (D * W) + 1e-06))
    input_step = input_factor * input_update
    gate_step = gate_factor * gate_update
    input_new = input_weight - learn_rate * input_step
    gate_new = gate_weight - learn_rate * gate_step
    input_copy, gate_copy = in_one_piece(
        (input_new.astype(jnp.bfloat16), gate_new.astype(jnp.bfloat16)), FS, 0, 1
    )
    return (
        input_new,
        gate_new,
        input_step,
        gate_step,
        in_first,
        in_second,
        gt_first,
        gt_second,
        input_copy,
        gate_copy,
    )


def solution(mesh):
    torus = Mesh(mesh.devices.reshape(8, 4, 4, 2), ("fs_0", "fs_1", "tp_0", "tp_1"))
    in_specs = (
        P(FS, None),
        P(FS, TP),
        P(FS, TP),
        P(FS, TP),
        P(FS, TP),
        P(FS, None),
        P(FS, None),
        P(FS, TP),
        P(FS, TP),
        P(FS, TP),
        P(FS, TP),
    )
    out_specs = (
        P(FS, TP),
        P(FS, TP),
        P(FS, TP),
        P(FS, TP),
        P(FS, TP),
        P(FS, TP),
        P(FS, TP),
        P(FS, TP),
        P(None, TP),
        P(None, TP),
    )
    return jax.shard_map(
        shards, mesh=torus, in_specs=in_specs, out_specs=out_specs, check_vma=False
    )
```

profile of v0, /device:TPU:1, one launch (start us, length us, event | category | flops | bytes accessed | tf_op | source)
XLA Modules:
  0.0 292.1 jit_solution(9906296930133326096)
XLA Ops:
  7.2 1.5 pad_maximum_fusion.1
  8.8 0.0 all-gather.5.cloned.1.call-start
  8.8 79.5 %all-gather.3.cloned.1.call-done = bf16[2048,512]{1,0:T(8,128)(2,1)} async-done(((bf16[64,512]{1,0:T(8,128)(2,1)}), bf16[2048,512]{1,0:T(8,128)(2,1)}) %all-gather.3.cloned.1.call-update) | async-done | bytes 2097168 | tf_op jit(solution)/shard_map/all_gather | solution.py:24
  88.3 6.2 %convolution_bitcast_fusion.1 = f32[2048,256]{0,1:T(8,128)S(1)} fusion(bf16[2048,2048]{1,0:T(8,128)(2,1)} %param.11, bf16[2048,512]{1,0:T(8,128)(2,1)} %all-gather.3.cloned.1.call-done), kind=kOutput, calls=%fused_computation.1 | convolution fusion | flops 2147483648 | bytes 11534336 | tf_op jit(solution)/shard_map/dot_general | solution.py:82
  94.6 0.5 fusion.8
  95.1 0.5 fusion
  95.7 1.0 copy-done.11
  96.7 2.4 convolution_bitcast_fusion
  99.1 0.5 fusion.5
  99.7 0.5 fusion.1
  100.3 0.1 copy.21
  100.4 15.7 %all_to_all.5 = bf16[32,8,512]{2,1,0:T(8,128)(2,1)S(1)} all-to-all(bf16[32,8,512]{2,1,0:T(8,128)(2,1)S(1)} %bitcast.19), channel_id=1, replica_groups=mesh['fs_0'=8,'fs_1'=4,'tp_0'=4,'tp_1'=2] {'fs_0','fs_1'}, dimensions={0} | all-to-all | bytes 524288 | tf_op jit(solution)/shard_map/all_to_all | solution.py:35
  116.3 0.6 divide_convert_fusion.1
  116.9 35.4 %all_gather.10 = bf16[256,512]{1,0:T(8,128)(2,1)S(1)} all-gather(bf16[8,512]{1,0:T(8,128)(2,1)S(1)} %pad_maximum_fusion.3), channel_id=1, replica_groups=mesh['fs_0'=8,'fs_1'=4,'tp_0'=4,'tp_1'=2] {'fs_0','fs_1'}, dimensions={0}, use_global_device_ids=true | all-gather | bytes 270336 | tf_op jit(solution)/shard_map/all_gather | solution.py:24
  152.3 0.8 multiply_reduce_fusion.1
  153.1 0.8 multiply_reduce_fusion
  153.9 13.5 %all-reduce = (f32[]{:T(128)}, f32[]{:T(128)}) all-reduce(f32[]{:T(128)} %get-tuple-element.35, f32[]{:T(128)} %get-tuple-element.37), channel_id=1, replica_groups=mesh['fs_0'=8,'fs_1'=4,'tp_0'=4,'tp_1'=2] {'fs_0'}, use_global_device_ids=true, to_apply=%region_2.0 | all-reduce | flops 2 | bytes 16 | tf_op jit(solution)/shard_map/psum | solution.py:49
  167.3 7.1 %all-reduce.2 = (f32[]{:T(128)}, f32[]{:T(128)}) all-reduce(f32[]{:T(128)} %get-tuple-element.10, f32[]{:T(128)} %get-tuple-element.11), channel_id=1, replica_groups=mesh['fs_0'=8,'fs_1'=4,'tp_0'=4,'tp_1'=2] {'fs_1'}, use_global_device_ids=true, to_apply=%region_3.0 | all-reduce | flops 2 | bytes 16 | tf_op jit(solution)/shard_map/psum | solution.py:49
  174.4 9.0 %all-reduce.1 = (f32[]{:T(128)}, f32[]{:T(128)}) all-reduce(f32[]{:T(128)} %get-tuple-element.14, f32[]{:T(128)} %get-tuple-element.15), channel_id=1, replica_groups=mesh['fs_0'=8,'fs_1'=4,'tp_0'=4,'tp_1'=2] {'tp_0'}, use_global_device_ids=true, to_apply=%region_4.0 | all-reduce | flops 2 | bytes 16 | tf_op jit(solution)/shard_map/psum | solution.py:49
  183.4 29.1 %all-reduce.3 = (f32[]{:T(128)}, f32[]{:T(128)}) all-reduce(f32[]{:T(128)} %get-tuple-element.12, f32[]{:T(128)} %get-tuple-element.13), channel_id=1, replica_groups=mesh['fs_0'=8,'fs_1'=4,'tp_0'=4,'tp_1'=2] {'tp_1'}, use_global_device_ids=true, to_apply=%region_5.0 | all-reduce | flops 2 | bytes 16 | tf_op jit(solution)/shard_map/psum | solution.py:49
  213.9 0.7 fusion.16
  214.6 0.6 pad_maximum_fusion.2
  215.3 67.0 %all-gather.5.cloned.1.call-done = bf16[2048,512]{1,0:T(8,128)(2,1)} async-done(((bf16[64,512]{1,0:T(8,128)(2,1)}), bf16[2048,512]{1,0:T(8,128)(2,1)}) %all-gather.5.cloned.1.call-update) | async-done | bytes 2097168 | tf_op jit(solution)/shard_map/all_gather | solution.py:24
  282.3 3.0 %fusion.20 = (bf16[2048,256]{1,0:T(8,128)(2,1)}, bf16[2048,256]{1,0:T(8,128)(2,1)}) fusion(bf16[2048,512]{1,0:T(8,128)(2,1)} %all-gather.5.cloned.1.call-done), kind=kLoop, calls=%fused_computation.41 | loop fusion | bytes 4194304 | tf_op jit(solution)/shard_map/split | solution.py:25
  (29 shorter events, 0.2 us)
Async XLA Ops:
  7.2 87.4 %copy-start = (bf16[2048,256]{1,0:T(8,128)(2,1)S(1)}, bf16[2048,256]{1,0:T(8,128)(2,1)}, u32[]{:S(2)}) copy-start(bf16[2048,256]{1,0:T(8,128)(2,1)} %param.12) | copy-start | bytes 3145732
  7.2 81.1 %all-gather.3.cloned.1.call-start = ((), (), s32[]{:S(2)}) async-start(), calls=%async_computation.1 | async-start | bytes 2162688 | tf_op jit(solution)/shard_map/all_gather | solution.py:24
  8.8 273.5 %all-gather.5.cloned.1.call-start = ((), (), s32[]{:S(2)}) async-start(), calls=%async_computation.2 | async-start | bytes 2162688 | tf_op jit(solution)/shard_map/all_gather | solution.py:24
  88.3 7.3 %copy-start.10 = (bf16[2048,2048]{1,0:T(8,128)(2,1)S(1)}, bf16[2048,2048]{1,0:T(8,128)(2,1)}, u32[]{:S(2)}) copy-start(bf16[2048,2048]{1,0:T(8,128)(2,1)} %param.11) | copy-start | bytes 25165828
  95.1 1.6 copy-start.11
  96.7 2.4 copy-start.1
  99.6 16.6 %copy-start.6 = (f32[8,256]{1,0:T(8,128)S(1)}, f32[8,256]{1,0:T(8,128)}, u32[]{:S(2)}) copy-start(f32[8,256]{1,0:T(8,128)} %param.19) | copy-start | bytes 24580
  99.6 16.6 %copy-start.7 = (f32[8,256]{1,0:T(8,128)S(1)}, f32[8,256]{1,0:T(8,128)}, u32[]{:S(2)}) copy-start(f32[8,256]{1,0:T(8,128)} %param.18) | copy-start | bytes 24580
  99.7 16.6 %copy-start.8 = (f32[8,256]{1,0:T(8,128)S(1)}, f32[8,256]{1,0:T(8,128)}, u32[]{:S(2)}) copy-start(f32[8,256]{1,0:T(8,128)} %param.21) | copy-start | bytes 24580
  99.7 16.6 %copy-start.9 = (f32[8,256]{1,0:T(8,128)S(1)}, f32[8,256]{1,0:T(8,128)}, u32[]{:S(2)}) copy-start(f32[8,256]{1,0:T(8,128)} %param.20) | copy-start | bytes 24580
  99.7 52.6 %copy-start.2 = (bf16[64,256]{1,0:T(8,128)(2,1)S(1)}, bf16[64,256]{1,0:T(8,128)(2,1)}, u32[]{:S(2)}) copy-start(bf16[64,256]{1,0:T(8,128)(2,1)} %param.16) | copy-start | bytes 98308
  100.2 52.9 %copy-start.3 = (bf16[64,256]{1,0:T(8,128)(2,1)S(1)}, bf16[64,256]{1,0:T(8,128)(2,1)}, u32[]{:S(2)}) copy-start(bf16[64,256]{1,0:T(8,128)(2,1)} %param.17) | copy-start | bytes 98308
  100.2 113.6 %copy-start.4 = (f32[64,256]{1,0:T(8,128)S(1)}, f32[64,256]{1,0:T(8,128)}, u32[]{:S(2)}) copy-start(f32[64,256]{1,0:T(8,128)} %param.14) | copy-start | bytes 196612
  100.3 113.6 %copy-start.5 = (f32[64,256]{1,0:T(8,128)S(1)}, f32[64,256]{1,0:T(8,128)}, u32[]{:S(2)}) copy-start(f32[64,256]{1,0:T(8,128)} %param.15) | copy-start | bytes 196612
Sparse Core Ops, SparseCore 0:
  11.2 77.1 all-gather.2
  215.4 66.8 all-gather.4
where the time goes:
time: 296 us; the launch traced here: 292 us
  waiting for transfers between devices  147 us (50%)
  blocking collectives  110 us (37%)
  between operations  15.6 us (5%)
  matrix products  12.3 us (4%)
  local copies, waits for them, and re-layouts  4.23 us (1%)
  other arithmetic  3.52 us (1%)
    all_gather x2, waiting for transfers between devices, in_one_piece(): filled = lax.all_gather(both, axis, axis=dim, tiled=True)  147 us
    psum x4, blocking collectives, by_axis(): return functools.reduce(lax.psum, axes, x)  58.7 us
    all_gather x1, blocking collectives, in_one_piece(): filled = lax.all_gather(both, axis, axis=dim, tiled=True)  35.4 us
    all_to_all x1, blocking collectives, sent_and_summed(): lax.all_to_all(blocks, axis, split_axis=0, concat_axis=0, tiled=True)  15.7 us
    dot_general x1, matrix products, shards(): jnp.dot(layer_input, pieces[0], preferred_element_type=jnp.float32)  6.23 us
  transfers between devices with their start and end apart: 2, of which 2 were waited for; matrix products, arithmetic and copies ran while one was open for 0% of the time, Pallas kernels for 0%

commit v1 on v0

v1 whole, which is shorter than its diff:
```python
import functools

import jax
import jax.numpy as jnp
from jax import lax
from jax.experimental import pallas as pl
from jax.experimental.pallas import tpu as pltpu
from jax.sharding import Mesh
from jax.sharding import PartitionSpec as P

FS = ("fs_0", "fs_1")
TP = ("tp_0", "tp_1")
MESH = pl.DeviceIdType.MESH
F32, BF16 = jnp.float32, jnp.bfloat16

first_decay = 0.8
second_decay = 0.95
learn_rate = 0.01


ARGS = ("x_in", "ci_in", "cg_in", "wi_in", "wg_in", "bi_in", "bg_in", "fi_in", "si_in", "fg_in", "sg_in")
OUTS = ("ni_out", "ng_out", "ti_out", "tg_out", "fi_out", "si_out", "fg_out", "sg_out", "ki_out", "kg_out")


def scratch(nz, ny, nx, tokens):
    rank, cols, rows = nz * ny * 8, 256, ny * 64
    vmem = {
        "xb": ((nz, tokens, rows), BF16),
        "cb": ((2, tokens, cols), BF16),
        "ct": ((2, cols, tokens), BF16),
        "gh": ((nz, 2, cols, rows), BF16),
        "gl": ((nz, 2, cols, rows), BF16),
        "st": ((2, cols, rank), F32),
        "bb": ((2, nz, ny, nx, 64 // nx, rank), BF16),
        "wf": ((2, 64, cols), F32),
        "wb": ((2, nz, ny, 64, cols), BF16),
        "mo": ((4, 8, cols), F32),
        "mn": ((4, 8, cols), F32),
        "sb": ((nz, ny, 16, cols), BF16),
        "ry": ((ny - 1, nz, 16, cols), BF16),
        "tz": ((nz, 16, cols), BF16),
        "rz": ((nz - 1, 16, cols), BF16),
        "db": ((nz, ny, 16, cols), BF16),
        "dd": ((2, rank, cols), BF16),
        "up": ((2, nz, rows, cols), F32),
        "ss": ((2 * nx, 8, 128), F32),
        "ob": ((2, 2, 64, cols), F32),
        "ck": ((2, nz, rows, cols), BF16),
    }
    sems = {
        "x_sem": (nz,), "c_sem": (2,), "w_sem": (2,), "b_sem": None, "m_sem": (4,), "out_sem": (10,),
        "z_recv": (nz,), "mid_recv": (nz,), "last_recv": (nz,), "core_recv": (nz,),
        "ring_recv": (2, 2, nz // 2 + 1), "wy_recv": None, "ay_recv": None, "az_recv": None,
        "dz_recv": None, "dy_recv": None, "ss_recv": None, "send": (11,),
    }
    names = tuple(vmem) + tuple(sems)
    dma = pltpu.SemaphoreType.DMA
    shapes = [pltpu.VMEM(*v) for v in vmem.values()] + [dma if v is None else dma(v) for v in sems.values()]
    return names, shapes


def update_kernel(nz, ny, nx, entries, names, *refs):
    r = dict(zip(ARGS + OUTS + names, refs))
    x_in, ci_in, cg_in, wi_in, wg_in, bi_in, bg_in, fi_in, si_in, fg_in, sg_in = (r[n] for n in ARGS)
    ni_out, ng_out, ti_out, tg_out, fi_out, si_out, fg_out, sg_out, ki_out, kg_out = (r[n] for n in OUTS)
    (
        xb, cb, ct, gh, gl, st, bb, wf, wb, mo, mn, sb, ry, tz, rz, db, dd, up, ss, ob, ck,
        x_sem, c_sem, w_sem, b_sem, m_sem, out_sem, z_recv, mid_recv, last_recv, core_recv,
        ring_recv, wy_recv, ay_recv, az_recv, dz_recv, dy_recv, ss_recv, send,
    ) = (r[n] for n in names)
    slab, rows, rank = 64 // nx, ny * 64, st.shape[2]
    z, y = lax.axis_index("fs_0"), lax.axis_index("fs_1")
    x, c = lax.axis_index("tp_0"), lax.axis_index("tp_1")
    me_tp = x * 2 + c
    own_l = y * (1 - c) + x * c
    own_m = x * (1 - c) + y * c

    def zz_of(k):
        sign = 2 * lax.rem(k, 2) - 1 if not isinstance(k, int) else 2 * (k % 2) - 1
        return lax.rem(z + sign * ((k + 1) // 2) + nz, nz)

    def peer_z(d):
        return {"fs_0": lax.rem(z + d, nz)}

    def peer_y(d):
        return {"fs_1": lax.rem(y + d, ny)}

    def peer_mid(d):
        return {"fs_1": lax.rem(y + d * c, ny), "tp_0": lax.rem(x + d * (1 - c), nx)}

    def peer_last(d):
        return {"fs_1": lax.rem(y + d * (1 - c), ny), "tp_0": lax.rem(x + d * c, nx)}

    def push(src, dst, s, recv, device):
        pltpu.make_async_remote_copy(
            src_ref=src, dst_ref=dst, send_sem=send.at[s], recv_sem=recv,
            device_id=device, device_id_type=MESH,
        ).start()

    def drain(ref, sem):
        pltpu.make_async_copy(ref, ref, sem).wait()

    def pull(src, dst, sem):
        pltpu.make_async_copy(src, dst, sem).start()

    barrier = pltpu.get_barrier_semaphore()
    peers = [peer_z(d) for d in range(1, nz)] + [peer_y(d) for d in range(1, ny)]
    peers += [{"tp_0": lax.rem(x + d, nx), "tp_1": cc} for d in range(1, nx) for cc in (0, 1)]
    peers += [{"tp_1": 1 - c}]
    for device in peers:
        pl.semaphore_signal(barrier, inc=1, device_id=device, device_id_type=MESH)

    @pl.when(c == 0)
    def _():
        pull(bi_in.at[pl.ds(x * slab, slab)], bb.at[0, z, y, x], b_sem)

    @pl.when(c == 1)
    def _():
        pull(bg_in.at[pl.ds(x * slab, slab)], bb.at[1, z, x, y], b_sem)

    pull(wi_in, wf.at[0], w_sem.at[0])
    pull(wg_in, wf.at[1], w_sem.at[1])
    pull(ci_in, cb.at[0], c_sem.at[0])
    pull(cg_in, cb.at[1], c_sem.at[1])
    for k in range(nz):
        zz = zz_of(k)
        pull(x_in.at[:, pl.ds(pl.multiple_of(zz * rows, 128), rows)], xb.at[k], x_sem.at[k])
    for i, ref in enumerate((fi_in, si_in, fg_in, sg_in)):
        pull(ref, mo.at[i], m_sem.at[i])

    for p in range(2):
        drain(wf.at[p], w_sem.at[p])
        wb[p, z, y] = wf[p].astype(BF16)
    drain(bb.at[c, z, own_l, own_m], b_sem)
    tokens = cb.shape[1]
    chunk = min(256, tokens)
    for p in range(2):
        drain(cb.at[p], c_sem.at[p])

        def flip(i, _):
            at = pl.ds(pl.multiple_of(i * chunk, chunk), chunk)
            ct[p, :, at] = cb[p, at, :].T
            return 0

        lax.fori_loop(0, tokens // chunk, flip, 0)

    pl.semaphore_wait(barrier, len(peers))

    def mid_sends(k):
        zz = zz_of(k)
        for d in range(1, nx):
            block = bb.at[c, zz, own_l, own_m]
            push(block, block, 1, mid_recv.at[k], peer_mid(d))

    def last_sends(k):
        zz = zz_of(k)
        for d in range(1, ny):
            block = bb.at[c, zz, own_l]
            push(block, block, 2, last_recv.at[k], peer_last(d))

    def z_duty(k):
        drain(bb.at[c, zz_of(k), own_l, own_m], z_recv.at[k])
        mid_sends(k)

    def mid_duty(k):
        drain(bb.at[c, zz_of(k), own_l, pl.ds(0, nx - 1)], mid_recv.at[k])
        last_sends(k)

    own = bb.at[c, z, own_l, own_m]
    for k in range(1, nz):
        sign, half = 2 * (k % 2) - 1, (k + 1) // 2
        at_peer = nz - 1 if k == nz - 1 else (k + 1 if k % 2 else k - 1)
        push(own, own, 0, z_recv.at[at_peer], peer_z((sign * half) % nz))
    mid_sends(0)
    for d in range(1, ny):
        push(wb.at[:, z, y], wb.at[:, z, y], 3, wy_recv, peer_y(d))

    def grad_step(k, _):
        drain(xb.at[k], x_sem.at[k])
        for p in range(2):
            g = jnp.dot(ct[p], xb[k], preferred_element_type=F32)
            hi = g.astype(BF16)
            gh[k, p] = hi
            gl[k, p] = (g - hi.astype(F32)).astype(BF16)

        @pl.when(k >= 2)
        def _():
            z_duty(k - 1)

        @pl.when(k >= 3)
        def _():
            mid_duty(k - 3)

        return 0

    lax.fori_loop(0, nz, grad_step, 0)
    for k in range(max(1, nz - 1), nz):
        z_duty(k)
    for k in range(max(0, nz - 3), nz):
        mid_duty(k)

    def ring_reach(p, way):
        return nz // 2 if p == way else nz - 1 - nz // 2

    def ring_block(p, way, s):
        return wb.at[p, lax.rem(z - s + nz if way == 0 else z + s, nz)]

    def ring_send(s):
        for p in range(2):
            for way in range(2):
                if s <= ring_reach(p, way):
                    block = ring_block(p, way, s - 1)
                    push(block, block, 4, ring_recv.at[p, way, s], peer_z(1 if way == 0 else nz - 1))

    def ring_wait(s):
        for p in range(2):
            for way in range(2):
                if s <= ring_reach(p, way):
                    drain(ring_block(p, way, s), ring_recv.at[p, way, s])

    drain(wb.at[:, z, pl.ds(0, ny - 1)], wy_recv)
    ring_send(1)

    def basis(p, j):
        if p == 0:
            return bb[0, j].reshape(rows, rank)
        b = bb[1, j]
        return jnp.concatenate([b[l, m] for m in range(ny) for l in range(nx)], axis=0)

    def core_send(k):
        zz = zz_of(k)
        drain(bb.at[c, zz, pl.ds(0, ny - 1)], last_recv.at[k])
        push(bb.at[c, zz], bb.at[c, zz], 5, core_recv.at[k], {"tp_1": 1 - c})

    def small_step(k):
        zz = zz_of(k)
        drain(bb.at[1 - c, zz], core_recv.at[k])
        for p in range(2):
            b = basis(p, zz)
            st[p] += jnp.dot(gh[k, p], b, preferred_element_type=F32) + jnp.dot(
                gl[k, p], b, preferred_element_type=F32
            )

    st[...] = jnp.zeros_like(st)
    core_send(0)

    def body(k, _):
        core_send(k + 1)
        small_step(k)
        return 0

    lax.fori_loop(0, nz - 1, body, 0)
    small_step(nz - 1)

    parts = [st[p].T.reshape(rank // 8, 8, st.shape[1]) for p in range(2)]
    sb[...] = jnp.concatenate(parts, axis=1).astype(BF16).reshape(sb.shape)
    for d in range(1, ny):
        yy = lax.rem(y + d, ny)
        push(sb.at[:, yy], ry.at[d - 1], 6, ay_recv, peer_y(d))
    if nz > 2:
        ring_wait(1)
        ring_send(2)
    drain(ry, ay_recv)
    total = sb[:, y].astype(F32)
    for d in range(1, ny):
        total += ry[d - 1].astype(F32)
    tz[...] = total.astype(BF16)
    for d in range(1, nz):
        push(tz.at[lax.rem(z + d, nz)], rz.at[d - 1], 7, az_recv, peer_z(d))
    drain(rz, az_recv)
    small = tz[z].astype(F32)
    for d in range(1, nz):
        small += rz[d - 1].astype(F32)

    for i in range(4):
        drain(mo.at[i], m_sem.at[i])
    first = jnp.concatenate([mo[0], mo[2]], axis=0)
    second = jnp.concatenate([mo[1], mo[3]], axis=0)
    first_new = first_decay * first + (1.0 - first_decay) * small
    second_new = second_decay * second + (1.0 - second_decay) * small * small
    db[z, y] = (first_new / (jnp.sqrt(second_new) + 1e-08)).astype(BF16)
    for d in range(1, nz):
        push(db.at[z, y], db.at[z, y], 8, dz_recv, peer_z(d))
    mn[0], mn[1] = first_new[:8], second_new[:8]
    mn[2], mn[3] = first_new[8:], second_new[8:]
    for i, ref in enumerate((fi_out, si_out, fg_out, sg_out)):
        pull(mn.at[i], ref, out_sem.at[i])
    if nz > 2:
        ring_wait(2)
        for s in (3,):
            if s <= nz // 2:
                ring_send(s)
    drain(db.at[pl.ds(0, nz - 1), y], dz_recv)
    for d in range(1, ny):
        push(db.at[:, y], db.at[:, y], 9, dy_recv, peer_y(d))
    if nz > 4:
        ring_wait(3)
        ring_send(4)
    drain(db.at[:, pl.ds(0, ny - 1)], dy_recv)

    directions = db[...].reshape(nz * ny, 16, db.shape[3]).astype(F32)
    halves = [directions[:, 8 * p : 8 * p + 8].reshape(rank, -1).astype(BF16) for p in range(2)]
    for p in range(2):
        dd[p] = halves[p]

    def update_step(j, sums):
        out = []
        for p in range(2):
            u = jnp.dot(basis(p, j), dd[p], preferred_element_type=F32)
            up[p, j] = u
            out.append(sums[p] + jnp.sum((u * u).reshape(-1, 8, u.shape[1]), axis=0))
        return tuple(out)

    zero = jnp.zeros((8, up.shape[3]), F32)
    sums = lax.fori_loop(0, nz, update_step, (zero, zero))
    row = lax.broadcasted_iota(jnp.int32, (8, 128), 0)
    ss[me_tp] = jnp.where(row == 0, jnp.sum(sums[0]), jnp.sum(sums[1]))
    mine = ss.at[me_tp]
    for d in range(1, nx):
        for cc in (0, 1):
            push(mine, mine, 10, ss_recv, {"tp_0": lax.rem(x + d, nx), "tp_1": cc})
    push(mine, mine, 10, ss_recv, {"tp_1": 1 - c})
    ring_wait(nz // 2)
    drain(ss.at[pl.ds(0, 2 * nx - 1)], ss_recv)
    squares = ss[0]
    for t in range(1, 2 * nx):
        squares += ss[t]
    factor = jnp.minimum(1.0, 1.0 / jnp.sqrt(squares / entries + 1e-06))
    factors = (factor[0, 0], factor[1, 0])

    def copy_step(j, _):
        for p in range(2):
            step = factors[p] * up[p, j]
            ck[p, j] = (wb[p, j].reshape(step.shape).astype(F32) - learn_rate * step).astype(BF16)
        for p, ref in enumerate((ki_out, kg_out)):
            pull(ck.at[p, j], ref.at[pl.ds(pl.multiple_of(j * rows, rows), rows)], out_sem.at[8 + p])
        return 0

    lax.fori_loop(0, nz, copy_step, 0)
    for p in range(2):
        step = factors[p] * up[p, z, pl.ds(pl.multiple_of(y * 64, 64), 64), :]
        ob[p, 0] = wf[p] - learn_rate * step
        ob[p, 1] = step
        pull(ob.at[p, 0], (ni_out, ng_out)[p], out_sem.at[4 + 2 * p])
        pull(ob.at[p, 1], (ti_out, tg_out)[p], out_sem.at[5 + 2 * p])
    for p in range(2):
        drain(ob.at[p, 0], out_sem.at[4 + 2 * p])
        drain(ob.at[p, 1], out_sem.at[5 + 2 * p])
        drain(ck.at[p], out_sem.at[8 + p])
    for i in range(4):
        drain(mn.at[i], out_sem.at[i])

    drain(bb.at[c, pl.ds(0, nz - 1), 0, 0], send.at[0])
    drain(bb.at[c, :, pl.ds(0, nx - 1), 0], send.at[1])
    drain(bb.at[c, :, pl.ds(0, ny - 1)], send.at[2])
    drain(wb.at[:, z, pl.ds(0, ny - 1)], send.at[3])
    drain(wb.at[:, pl.ds(0, nz - 1)], send.at[4])
    drain(bb.at[c], send.at[5])
    drain(ry, send.at[6])
    drain(rz, send.at[7])
    drain(db.at[pl.ds(0, nz - 1), 0], send.at[8])
    drain(db.at[:, pl.ds(0, ny - 1)], send.at[9])
    drain(ss.at[pl.ds(0, 2 * nx - 1)], send.at[10])


def shards(nz, ny, nx, entries, *args):
    names, shapes = scratch(nz, ny, nx, args[0].shape[0])
    w, m = args[3], args[7]
    copy = jax.ShapeDtypeStruct((w.shape[0] * nz * ny, w.shape[1]), BF16)
    outs = [jax.ShapeDtypeStruct(a.shape, F32) for a in (w,) * 4 + (m,) * 4] + [copy, copy]
    anywhere = pl.BlockSpec(memory_space=pl.ANY)
    return tuple(
        pl.pallas_call(
            functools.partial(update_kernel, nz, ny, nx, entries, names),
            out_shape=outs,
            in_specs=[anywhere] * len(args),
            out_specs=[anywhere] * len(outs),
            scratch_shapes=shapes,
            compiler_params=pltpu.CompilerParams(
                collective_id=0, has_side_effects=True, vmem_limit_bytes=56 * 1024 * 1024
            ),
        )(*args)
    )


def build(devices, nz, ny, nx):
    torus = Mesh(devices.reshape(nz, ny, nx, 2), FS + TP)
    entries = float(nz * ny * 64 * nx * 2 * 256)
    sharded, copied = P(FS, TP), P(None, TP)
    in_specs = (P(FS, None), sharded, sharded, sharded, sharded, P(FS, None), P(FS, None)) + (sharded,) * 4
    return jax.shard_map(
        functools.partial(shards, nz, ny, nx, entries),
        mesh=torus,
        in_specs=in_specs,
        out_specs=(sharded,) * 8 + (copied,) * 2,
        check_vma=False,
    )


def solution(mesh):
    return build(mesh.devices, 8, 4, 4)
```

time: 296 us -> 77 us (0.26); the launches traced: 292 us -> 76.5 us
  waiting for transfers between devices: 147 us -> 0 us
  blocking collectives: 110 us -> 0 us
  Pallas kernels: 0 us -> 60.2 us
  between operations: 15.6 us -> 0.66 us
  matrix products: 12.3 us -> 0 us
  local copies, waits for them, and re-layouts: 4.23 us -> 15.6 us
  other arithmetic: 3.52 us -> 0 us
    all_gather x2 -> x0, waiting for transfers between devices: 147 us -> none  [in_one_piece(): filled = lax.all_gather(both, axis, axis=dim, tiled=True)]
    pallas_call x0 -> x1, Pallas kernels: none -> 60.2 us  [shards(): pl.pallas_call(functools.partial(update_kernel, nz, ny, nx, entries, name...]
    psum x4 -> x0, blocking collectives: 58.7 us -> none  [by_axis(): return functools.reduce(lax.psum, axes, x)]
    all_gather x1 -> x0, blocking collectives: 35.4 us -> none  [in_one_piece(): filled = lax.all_gather(both, axis, axis=dim, tiled=True)]
    all_to_all x1 -> x0, blocking collectives: 15.7 us -> none  [sent_and_summed(): lax.all_to_all(blocks, axis, split_axis=0, concat_axis=0, tiled=True)]
    unnamed x24 -> x10, local copies, waits for them, and re-layouts: 1.1 us -> 15.6 us
    dot_general x8 -> x0, matrix products: 12.3 us -> none  [the longest x1 6.23 us: shards(): jnp.dot(layer_input, pieces[0], preferred_element_type=jnp.float32)]
    split x1 -> x0, local copies, waits for them, and re-layouts: 2.99 us -> none  [in_one_piece(): jnp.split(filled, [sum(widths[:k]) for k in range(1, len(widths))], axis=...]
  transfers between devices with their start and end apart: 2 -> 0, of which waited for: 2 -> 0; matrix products, arithmetic and copies ran while one was open for 0% -> 0% of each run, Pallas kernels for 0% -> 0%
where the time goes in v1:
time: 77 us; the launch traced here: 76.5 us
  Pallas kernels  60.2 us (78%)
  local copies, waits for them, and re-layouts  15.6 us (20%)
    pallas_call x1, Pallas kernels, shards(): pl.pallas_call(functools.partial(update_kernel, nz, ny, nx, entries, name...  60.2 us
    unnamed x10, local copies, waits for them, and re-layouts  15.6 us

profile of v1, /device:TPU:1, one launch (start us, length us, event | category | flops | bytes accessed | tf_op | source)
XLA Modules:
  0.0 76.5 jit_solution(16759305834120689504)
XLA Ops:
  0.6 60.2 %shard_map.186 = (f32[64,256]{1,0:T(8,128)}, f32[64,256]{1,0:T(8,128)}, f32[64,256]{1,0:T(8,128)}, f32[64,256]{1,0:T(8,128)}, f32[8,256]{1,0:T(8,128)}, /*index=...) custom-call(bf16[2048,2048]{1,0:T(8,128)(2,1)} %refs_0_.1, ...), custom_call_target="tpu_custom_call" | custom-call | tf_op jit(solution)/shard_map/pallas_call | solution.py:373
  60.9 1.5 %copy.31 = f32[64,256]{1,0:T(8,128)} copy(f32[64,256]{1,0:T(8,128)} %get-tuple-element.20) | data formatting | bytes 131072
  62.4 1.5 %copy.32 = f32[64,256]{1,0:T(8,128)} copy(f32[64,256]{1,0:T(8,128)} %get-tuple-element.21) | data formatting | bytes 131072
  63.8 1.5 %copy.33 = f32[64,256]{1,0:T(8,128)} copy(f32[64,256]{1,0:T(8,128)} %get-tuple-element.22) | data formatting | bytes 131072
  65.3 1.5 %copy.34 = f32[64,256]{1,0:T(8,128)} copy(f32[64,256]{1,0:T(8,128)} %get-tuple-element.23) | data formatting | bytes 131072
  66.8 1.3 %copy.35 = f32[8,256]{1,0:T(8,128)} copy(f32[8,256]{1,0:T(8,128)} %get-tuple-element.24) | data formatting | bytes 16384
  68.1 1.3 %copy.36 = f32[8,256]{1,0:T(8,128)} copy(f32[8,256]{1,0:T(8,128)} %get-tuple-element.25) | data formatting | bytes 16384
  69.4 1.3 %copy.37 = f32[8,256]{1,0:T(8,128)} copy(f32[8,256]{1,0:T(8,128)} %get-tuple-element.26) | data formatting | bytes 16384
  70.7 1.3 %copy.38 = f32[8,256]{1,0:T(8,128)} copy(f32[8,256]{1,0:T(8,128)} %get-tuple-element.27) | data formatting | bytes 16384
  72.0 2.3 %copy.39 = bf16[2048,256]{1,0:T(8,128)(2,1)} copy(bf16[2048,256]{1,0:T(8,128)(2,1)} %get-tuple-element.28) | data formatting | bytes 2097152
  74.2 2.3 %copy.40 = bf16[2048,256]{1,0:T(8,128)(2,1)} copy(bf16[2048,256]{1,0:T(8,128)(2,1)} %get-tuple-element.29) | data formatting | bytes 2097152

commit v2 on v1

--- a/solution.py
+++ b/solution.py
@@ -19,6 +19,7 @@
 
 
 ARGS = ("x_in", "ci_in", "cg_in", "wi_in", "wg_in", "bi_in", "bg_in", "fi_in", "si_in", "fg_in", "sg_in")
+HELD = ("up", "wb", "wf", "mn", "factor")
 OUTS = ("ni_out", "ng_out", "ti_out", "tg_out", "fi_out", "si_out", "fg_out", "sg_out", "ki_out", "kg_out")
 
 
@@ -32,40 +33,41 @@
         "gl": ((nz, 2, cols, rows), BF16),
         "st": ((2, cols, rank), F32),
         "bb": ((2, nz, ny, nx, 64 // nx, rank), BF16),
-        "wf": ((2, 64, cols), F32),
-        "wb": ((2, nz, ny, 64, cols), BF16),
         "mo": ((4, 8, cols), F32),
-        "mn": ((4, 8, cols), F32),
         "sb": ((nz, ny, 16, cols), BF16),
         "ry": ((ny - 1, nz, 16, cols), BF16),
         "tz": ((nz, 16, cols), BF16),
         "rz": ((nz - 1, 16, cols), BF16),
         "db": ((nz, ny, 16, cols), BF16),
         "dd": ((2, rank, cols), BF16),
-        "up": ((2, nz, rows, cols), F32),
         "ss": ((2 * nx, 8, 128), F32),
-        "ob": ((2, 2, 64, cols), F32),
-        "ck": ((2, nz, rows, cols), BF16),
     }
     sems = {
-        "x_sem": (nz,), "c_sem": (2,), "w_sem": (2,), "b_sem": None, "m_sem": (4,), "out_sem": (10,),
+        "x_sem": (nz,), "c_sem": (2,), "w_sem": (2,), "b_sem": None, "m_sem": (4,),
         "z_recv": (nz,), "mid_recv": (nz,), "last_recv": (nz,), "core_recv": (nz,),
         "ring_recv": (2, 2, nz // 2 + 1), "wy_recv": None, "ay_recv": None, "az_recv": None,
         "dz_recv": None, "dy_recv": None, "ss_recv": None, "send": (11,),
     }
+    held = {
+        "up": ((2, nz, rows, cols), F32),
+        "wb": ((2, nz, ny, 64, cols), BF16),
+        "wf": ((2, 64, cols), F32),
+        "mn": ((4, 8, cols), F32),
+        "factor": ((8, 128), F32),
+    }
     names = tuple(vmem) + tuple(sems)
     dma = pltpu.SemaphoreType.DMA
     shapes = [pltpu.VMEM(*v) for v in vmem.values()] + [dma if v is None else dma(v) for v in sems.values()]
-    return names, shapes
+    return names, shapes, [pltpu.VMEM(*v) for v in held.values()]
 
 
 def update_kernel(nz, ny, nx, entries, names, *refs):
-    r = dict(zip(ARGS + OUTS + names, refs))
+    r = dict(zip(ARGS + HELD + names, refs))
     x_in, ci_in, cg_in, wi_in, wg_in, bi_in, bg_in, fi_in, si_in, fg_in, sg_in = (r[n] for n in ARGS)
-    ni_out, ng_out, ti_out, tg_out, fi_out, si_out, fg_out, sg_out, ki_out, kg_out = (r[n] for n in OUTS)
+    up, wb, wf, mn, factor = (r[n] for n in HELD)
     (
-        xb, cb, ct, gh, gl, st, bb, wf, wb, mo, mn, sb, ry, tz, rz, db, dd, up, ss, ob, ck,
-        x_sem, c_sem, w_sem, b_sem, m_sem, out_sem, z_recv, mid_recv, last_recv, core_recv,
+        xb, cb, ct, gh, gl, st, bb, mo, sb, ry, tz, rz, db, dd, ss,
+        x_sem, c_sem, w_sem, b_sem, m_sem, z_recv, mid_recv, last_recv, core_recv,
         ring_recv, wy_recv, ay_recv, az_recv, dz_recv, dy_recv, ss_recv, send,
     ) = (r[n] for n in names)
     slab, rows, rank = 64 // nx, ny * 64, st.shape[2]
@@ -283,8 +285,6 @@
         push(db.at[z, y], db.at[z, y], 8, dz_recv, peer_z(d))
     mn[0], mn[1] = first_new[:8], second_new[:8]
     mn[2], mn[3] = first_new[8:], second_new[8:]
-    for i, ref in enumerate((fi_out, si_out, fg_out, sg_out)):
-        pull(mn.at[i], ref, out_sem.at[i])
     if nz > 2:
         ring_wait(2)
         for s in (3,):
@@ -325,30 +325,7 @@
     squares = ss[0]
     for t in range(1, 2 * nx):
         squares += ss[t]
-    factor = jnp.minimum(1.0, 1.0 / jnp.sqrt(squares / entries + 1e-06))
-    factors = (factor[0, 0], factor[1, 0])
-
-    def copy_step(j, _):
-        for p in range(2):
-            step = factors[p] * up[p, j]
-            ck[p, j] = (wb[p, j].reshape(step.shape).astype(F32) - learn_rate * step).astype(BF16)
-        for p, ref in enumerate((ki_out, kg_out)):
-            pull(ck.at[p, j], ref.at[pl.ds(pl.multiple_of(j * rows, rows), rows)], out_sem.at[8 + p])
-        return 0
-
-    lax.fori_loop(0, nz, copy_step, 0)
-    for p in range(2):
-        step = factors[p] * up[p, z, pl.ds(pl.multiple_of(y * 64, 64), 64), :]
-        ob[p, 0] = wf[p] - learn_rate * step
-        ob[p, 1] = step
-        pull(ob.at[p, 0], (ni_out, ng_out)[p], out_sem.at[4 + 2 * p])
-        pull(ob.at[p, 1], (ti_out, tg_out)[p], out_sem.at[5 + 2 * p])
-    for p in range(2):
-        drain(ob.at[p, 0], out_sem.at[4 + 2 * p])
-        drain(ob.at[p, 1], out_sem.at[5 + 2 * p])
-        drain(ck.at[p], out_sem.at[8 + p])
-    for i in range(4):
-        drain(mn.at[i], out_sem.at[i])
+    factor[...] = jnp.minimum(1.0, 1.0 / jnp.sqrt(squares / entries + 1e-06))
 
     drain(bb.at[c, pl.ds(0, nz - 1), 0, 0], send.at[0])
     drain(bb.at[c, :, pl.ds(0, nx - 1), 0], send.at[1])
@@ -363,23 +340,68 @@
     drain(ss.at[pl.ds(0, 2 * nx - 1)], send.at[10])
 
 
+def finish_kernel(nz, ny, up, wb, wf, mn, factor, *refs):
+    outs, (ob, ck, sem) = refs[:10], refs[10:]
+    z, y = lax.axis_index("fs_0"), lax.axis_index("fs_1")
+    rows = up.shape[2]
+    factors = (factor[0, 0], factor[1, 0])
+
+    def put(src, dst, k):
+        pltpu.make_async_copy(src, dst, sem.at[k]).start()
+
+    for i in range(4):
+        put(mn.at[i], outs[4 + i], 4 + i)
+    for p in range(2):
+        step = factors[p] * up[p, z, pl.ds(pl.multiple_of(y * 64, 64), 64), :]
+        ob[p] = wf[p] - learn_rate * step
+        ob[2 + p] = step
+    for i in range(4):
+        put(ob.at[i], outs[i], i)
+
+    def copy_step(j, _):
+        for p in range(2):
+            step = factors[p] * up[p, j]
+            ck[p, j] = (wb[p, j].reshape(step.shape).astype(F32) - learn_rate * step).astype(BF16)
+            put(ck.at[p, j], outs[8 + p].at[pl.ds(pl.multiple_of(j * rows, rows), rows)], 8 + p)
+        return 0
+
+    lax.fori_loop(0, nz, copy_step, 0)
+    for i in range(4):
+        pltpu.make_async_copy(mn.at[i], outs[4 + i], sem.at[4 + i]).wait()
+        pltpu.make_async_copy(ob.at[i], outs[i], sem.at[i]).wait()
+    for p in range(2):
+        pltpu.make_async_copy(ck.at[p], ck.at[p], sem.at[8 + p]).wait()
+
+
 def shards(nz, ny, nx, entries, *args):
-    names, shapes = scratch(nz, ny, nx, args[0].shape[0])
+    names, shapes, held = scratch(nz, ny, nx, args[0].shape[0])
+    hbm, vmem = pl.BlockSpec(memory_space=pltpu.HBM), pl.BlockSpec(memory_space=pltpu.VMEM)
+    kept = pl.pallas_call(
+        functools.partial(update_kernel, nz, ny, nx, entries, names),
+        out_shape=held,
+        in_specs=[hbm] * len(args),
+        out_specs=[vmem] * len(held),
+        scratch_shapes=shapes,
+        compiler_params=pltpu.CompilerParams(
+            collective_id=0, has_side_effects=True, vmem_limit_bytes=58 * 1024 * 1024 - 448 * 1024
+        ),
+    )(*args)
     w, m = args[3], args[7]
     copy = jax.ShapeDtypeStruct((w.shape[0] * nz * ny, w.shape[1]), BF16)
     outs = [jax.ShapeDtypeStruct(a.shape, F32) for a in (w,) * 4 + (m,) * 4] + [copy, copy]
-    anywhere = pl.BlockSpec(memory_space=pl.ANY)
     return tuple(
         pl.pallas_call(
-            functools.partial(update_kernel, nz, ny, nx, entries, names),
+            functools.partial(finish_kernel, nz, ny),
             out_shape=outs,
-            in_specs=[anywhere] * len(args),
-            out_specs=[anywhere] * len(outs),
-            scratch_shapes=shapes,
-            compiler_params=pltpu.CompilerParams(
-                collective_id=0, has_side_effects=True, vmem_limit_bytes=56 * 1024 * 1024
-            ),
-        )(*args)
+            in_specs=[vmem] * len(kept),
+            out_specs=[hbm] * len(outs),
+            scratch_shapes=[
+                pltpu.VMEM((4,) + w.shape, F32),
+                pltpu.VMEM((2, nz, ny * 64, w.shape[1]), BF16),
+                pltpu.SemaphoreType.DMA((10,)),
+            ],
+            compiler_params=pltpu.CompilerParams(vmem_limit_bytes=16 * 1024 * 1024),
+        )(*kept)
     )
 
 

time: 77 us -> 60.8 us (0.79)
  local copies, waits for them, and re-layouts: 15.6 us -> 0 us
    unnamed x10 -> x0, local copies, waits for them, and re-layouts: 15.6 us -> none
    pallas_call x1, Pallas kernels: 60.2 us -> 58.6 us  [shards(): pl.pallas_call(functools.partial(update_kernel, nz, ny, nx, entries, name...]
    pallas_call x0 -> x1, Pallas kernels: none -> 1.52 us  [shards(): pl.pallas_call(functools.partial(finish_kernel, nz, ny), out_shape=outs,...]
where the time goes in v2:
time: 60.8 us
  Pallas kernels  60.1 us (99%)
  between operations  0.65 us (1%)
    pallas_call x1, Pallas kernels, shards(): pl.pallas_call(functools.partial(update_kernel, nz, ny, nx, entries, name...  58.6 us
    pallas_call x1, Pallas kernels, shards(): pl.pallas_call(functools.partial(finish_kernel, nz, ny), out_shape=outs,...  1.52 us

profile of v2, /device:TPU:1, one launch (start us, length us, event | category | flops | bytes accessed | tf_op | source)
XLA Modules:
  0.0 60.8 jit_solution(4893813483620189533)
XLA Ops:
  0.6 58.6 %shard_map.186 = (f32[2,8,256,256]{3,2,1,0:T(8,128)S(1)}, bf16[2,8,4,64,256]{4,3,2,1,0:T(8,128)(2,1)S(1)}, f32[2,64,256]{2,1,0:T(8,128)S(1)}, f32[4,8,256]{2,1,0:T(8,128)S(1)}, f32[8,128]{1,0:T(8,128)S(1)}) custom-call(bf16[2048,2048]{1,0:T(8,128)(2,1)} %refs_0_.1, bf16[2048,256]{1,0:T(8,128)(2,1)} %refs_1_.1, bf16[2048,256]{1,0:T(8,128)(2,1)} %refs_2_.1, ...), custom_call_target="tpu_custom_call" | custom-call | tf_op jit(solution)/shard_map/pallas_call | solution.py:379
  59.2 1.5 %shard_map.187 = (f32[64,256]{1,0:T(8,128)}, f32[64,256]{1,0:T(8,128)}, f32[64,256]{1,0:T(8,128)}, f32[64,256]{1,0:T(8,128)}, f32[8,256]{1,0:T(8,128)}, /*index=...) custom-call(f32[2,8,256,256]{3,2,1,0:T(8,128)S(1)} %get-tuple-elemen, ...), custom_call_target="tpu_custom_call" | custom-call | tf_op jit(solution)/shard_map/pallas_call | solution.py:393

commit v3 on v2

--- a/solution.py
+++ b/solution.py
@@ -40,6 +40,8 @@
         "rz": ((nz - 1, 16, cols), BF16),
         "db": ((nz, ny, 16, cols), BF16),
         "dd": ((2, rank, cols), BF16),
+        "gm": ((2, rank, rank), F32),
+        "gb": ((2, 2, rank, rank), BF16),
         "ss": ((2 * nx, 8, 128), F32),
     }
     sems = {
@@ -66,7 +68,7 @@
     x_in, ci_in, cg_in, wi_in, wg_in, bi_in, bg_in, fi_in, si_in, fg_in, sg_in = (r[n] for n in ARGS)
     up, wb, wf, mn, factor = (r[n] for n in HELD)
     (
-        xb, cb, ct, gh, gl, st, bb, mo, sb, ry, tz, rz, db, dd, ss,
+        xb, cb, ct, gh, gl, st, bb, mo, sb, ry, tz, rz, db, dd, gm, gb, ss,
         x_sem, c_sem, w_sem, b_sem, m_sem, z_recv, mid_recv, last_recv, core_recv,
         ring_recv, wy_recv, ay_recv, az_recv, dz_recv, dy_recv, ss_recv, send,
     ) = (r[n] for n in names)
@@ -77,6 +79,9 @@
     own_l = y * (1 - c) + x * c
     own_m = x * (1 - c) + y * c
 
+    def far_first(n):
+        return sorted(range(1, n), key=lambda d: -min(d, n - d))
+
     def zz_of(k):
         sign = 2 * lax.rem(k, 2) - 1 if not isinstance(k, int) else 2 * (k % 2) - 1
         return lax.rem(z + sign * ((k + 1) // 2) + nz, nz)
@@ -150,13 +155,13 @@
 
     def mid_sends(k):
         zz = zz_of(k)
-        for d in range(1, nx):
+        for d in far_first(nx):
             block = bb.at[c, zz, own_l, own_m]
             push(block, block, 1, mid_recv.at[k], peer_mid(d))
 
     def last_sends(k):
         zz = zz_of(k)
-        for d in range(1, ny):
+        for d in far_first(ny):
             block = bb.at[c, zz, own_l]
             push(block, block, 2, last_recv.at[k], peer_last(d))
 
@@ -169,12 +174,12 @@
         last_sends(k)
 
     own = bb.at[c, z, own_l, own_m]
-    for k in range(1, nz):
+    for k in range(nz - 1, 0, -1):
         sign, half = 2 * (k % 2) - 1, (k + 1) // 2
         at_peer = nz - 1 if k == nz - 1 else (k + 1 if k % 2 else k - 1)
         push(own, own, 0, z_recv.at[at_peer], peer_z((sign * half) % nz))
     mid_sends(0)
-    for d in range(1, ny):
+    for d in far_first(ny):
         push(wb.at[:, z, y], wb.at[:, z, y], 3, wy_recv, peer_y(d))
 
     def grad_step(k, _):
@@ -184,22 +189,23 @@
             hi = g.astype(BF16)
             gh[k, p] = hi
             gl[k, p] = (g - hi.astype(F32)).astype(BF16)
-
-        @pl.when(k >= 2)
-        def _():
-            z_duty(k - 1)
-
-        @pl.when(k >= 3)
-        def _():
-            mid_duty(k - 3)
-
         return 0
 
-    lax.fori_loop(0, nz, grad_step, 0)
-    for k in range(max(1, nz - 1), nz):
-        z_duty(k)
-    for k in range(max(0, nz - 3), nz):
-        mid_duty(k)
+    def each(first, last, duty):
+        def one(k, _):
+            duty(k)
+            return 0
+
+        lax.fori_loop(first, last, one, 0)
+
+    cut1, cut2 = (nz * 5) // 8, (nz * 6) // 8
+    lax.fori_loop(0, cut1, grad_step, 0)
+    each(1, cut1, z_duty)
+    mid_duty(0)
+    lax.fori_loop(cut1, cut2, grad_step, 0)
+    each(cut1, nz, z_duty)
+    lax.fori_loop(cut2, nz, grad_step, 0)
+    each(1, nz, mid_duty)
 
     def ring_reach(p, way):
         return nz // 2 if p == way else nz - 1 - nz // 2
@@ -256,18 +262,33 @@
 
     parts = [st[p].T.reshape(rank // 8, 8, st.shape[1]) for p in range(2)]
     sb[...] = jnp.concatenate(parts, axis=1).astype(BF16).reshape(sb.shape)
-    for d in range(1, ny):
+    for d in far_first(ny):
         yy = lax.rem(y + d, ny)
         push(sb.at[:, yy], ry.at[d - 1], 6, ay_recv, peer_y(d))
     if nz > 2:
         ring_wait(1)
         ring_send(2)
+
+    gm[...] = jnp.zeros_like(gm)
+
+    def gram_step(j, _):
+        for p in range(2):
+            b = bb[p, j].reshape(rows, rank)
+            gm[p] += lax.dot_general(b, b, (((0,), (0,)), ((), ())), preferred_element_type=F32)
+        return 0
+
+    lax.fori_loop(0, nz, gram_step, 0)
+    for p in range(2):
+        gram = gm[p]
+        hi = gram.astype(BF16)
+        gb[p, 0] = hi
+        gb[p, 1] = (gram - hi.astype(F32)).astype(BF16)
     drain(ry, ay_recv)
     total = sb[:, y].astype(F32)
     for d in range(1, ny):
         total += ry[d - 1].astype(F32)
     tz[...] = total.astype(BF16)
-    for d in range(1, nz):
+    for d in far_first(nz):
         push(tz.at[lax.rem(z + d, nz)], rz.at[d - 1], 7, az_recv, peer_z(d))
     drain(rz, az_recv)
     small = tz[z].astype(F32)
@@ -281,7 +302,7 @@
     first_new = first_decay * first + (1.0 - first_decay) * small
     second_new = second_decay * second + (1.0 - second_decay) * small * small
     db[z, y] = (first_new / (jnp.sqrt(second_new) + 1e-08)).astype(BF16)
-    for d in range(1, nz):
+    for d in far_first(nz):
         push(db.at[z, y], db.at[z, y], 8, dz_recv, peer_z(d))
     mn[0], mn[1] = first_new[:8], second_new[:8]
     mn[2], mn[3] = first_new[8:], second_new[8:]
@@ -291,7 +312,7 @@
             if s <= nz // 2:
                 ring_send(s)
     drain(db.at[pl.ds(0, nz - 1), y], dz_recv)
-    for d in range(1, ny):
+    for d in far_first(ny):
         push(db.at[:, y], db.at[:, y], 9, dy_recv, peer_y(d))
     if nz > 4:
         ring_wait(3)
@@ -299,27 +320,27 @@
     drain(db.at[:, pl.ds(0, ny - 1)], dy_recv)
 
     directions = db[...].reshape(nz * ny, 16, db.shape[3]).astype(F32)
-    halves = [directions[:, 8 * p : 8 * p + 8].reshape(rank, -1).astype(BF16) for p in range(2)]
-    for p in range(2):
-        dd[p] = halves[p]
-
-    def update_step(j, sums):
-        out = []
-        for p in range(2):
-            u = jnp.dot(basis(p, j), dd[p], preferred_element_type=F32)
-            up[p, j] = u
-            out.append(sums[p] + jnp.sum((u * u).reshape(-1, 8, u.shape[1]), axis=0))
-        return tuple(out)
-
-    zero = jnp.zeros((8, up.shape[3]), F32)
-    sums = lax.fori_loop(0, nz, update_step, (zero, zero))
+    sums = []
+    for p in range(2):
+        d32 = directions[:, 8 * p : 8 * p + 8].reshape(rank, -1)
+        dd[p] = d32.astype(BF16)
+        q = jnp.dot(gb[p, 0], dd[p], preferred_element_type=F32)
+        q += jnp.dot(gb[p, 1], dd[p], preferred_element_type=F32)
+        sums.append(jnp.maximum(jnp.sum(q * d32), 0.0))
     row = lax.broadcasted_iota(jnp.int32, (8, 128), 0)
-    ss[me_tp] = jnp.where(row == 0, jnp.sum(sums[0]), jnp.sum(sums[1]))
+    ss[me_tp] = jnp.where(row == 0, sums[0], sums[1])
     mine = ss.at[me_tp]
-    for d in range(1, nx):
+    for d in far_first(nx):
         for cc in (0, 1):
             push(mine, mine, 10, ss_recv, {"tp_0": lax.rem(x + d, nx), "tp_1": cc})
     push(mine, mine, 10, ss_recv, {"tp_1": 1 - c})
+
+    def update_step(j, _):
+        for p in range(2):
+            up[p, j] = jnp.dot(basis(p, j), dd[p], preferred_element_type=F32)
+        return 0
+
+    lax.fori_loop(0, nz, update_step, 0)
     ring_wait(nz // 2)
     drain(ss.at[pl.ds(0, 2 * nx - 1)], ss_recv)
     squares = ss[0]

time: 60.8 us -> 55.2 us (0.908)
  Pallas kernels: 60.1 us -> 54.5 us
    pallas_call x1, Pallas kernels: 58.6 us -> 52.9 us  [shards(): pl.pallas_call(functools.partial(update_kernel, nz, ny, nx, entries, name...]
where the time goes in v3:
time: 55.2 us; the launch traced here: 55.1 us
  Pallas kernels  54.5 us (99%)
  between operations  0.65 us (1%)
    pallas_call x1, Pallas kernels, shards(): pl.pallas_call(functools.partial(update_kernel, nz, ny, nx, entries, name...  52.9 us
    pallas_call x1, Pallas kernels, shards(): pl.pallas_call(functools.partial(finish_kernel, nz, ny), out_shape=outs,...  1.52 us

profile of v3, /device:TPU:1, one launch (start us, length us, event | category | flops | bytes accessed | tf_op | source)
XLA Modules:
  0.0 55.1 jit_solution(161837856403164073)
XLA Ops:
  0.6 52.9 %shard_map.186 = (f32[2,8,256,256]{3,2,1,0:T(8,128)S(1)}, bf16[2,8,4,64,256]{4,3,2,1,0:T(8,128)(2,1)S(1)}, f32[2,64,256]{2,1,0:T(8,128)S(1)}, f32[4,8,256]{2,1,0:T(8,128)S(1)}, f32[8,128]{1,0:T(8,128)S(1)}) custom-call(bf16[2048,2048]{1,0:T(8,128)(2,1)} %refs_0_.1, bf16[2048,256]{1,0:T(8,128)(2,1)} %refs_1_.1, bf16[2048,256]{1,0:T(8,128)(2,1)} %refs_2_.1, ...), custom_call_target="tpu_custom_call" | custom-call | tf_op jit(solution)/shard_map/pallas_call | solution.py:400
  53.6 1.5 %shard_map.187 = (f32[64,256]{1,0:T(8,128)}, f32[64,256]{1,0:T(8,128)}, f32[64,256]{1,0:T(8,128)}, f32[64,256]{1,0:T(8,128)}, f32[8,256]{1,0:T(8,128)}, /*index=...) custom-call(f32[2,8,256,256]{3,2,1,0:T(8,128)S(1)} %get-tuple-elemen, ...), custom_call_target="tpu_custom_call" | custom-call | tf_op jit(solution)/shard_map/pallas_call | solution.py:414

commit v4 on v3

--- a/solution.py
+++ b/solution.py
@@ -29,8 +29,8 @@
         "xb": ((nz, tokens, rows), BF16),
         "cb": ((2, tokens, cols), BF16),
         "ct": ((2, cols, tokens), BF16),
-        "gh": ((nz, 2, cols, rows), BF16),
-        "gl": ((nz, 2, cols, rows), BF16),
+        "gg": ((nz, 2, 2, cols, rows), BF16),
+        "gp": ((nz, 2, cols, rows), BF16),
         "st": ((2, cols, rank), F32),
         "bb": ((2, nz, ny, nx, 64 // nx, rank), BF16),
         "mo": ((4, 8, cols), F32),
@@ -40,22 +40,26 @@
         "rz": ((nz - 1, 16, cols), BF16),
         "db": ((nz, ny, 16, cols), BF16),
         "dd": ((2, rank, cols), BF16),
-        "gm": ((2, rank, rank), F32),
-        "gb": ((2, 2, rank, rank), BF16),
+        "gm": ((rank, rank), F32),
+        "gb": ((2, rank, rank), BF16),
+        "pm": ((2, 8, cols), F32),
+        "pn": ((2, 8, cols), F32),
+        "dp": ((rank, cols), BF16),
         "ss": ((2 * nx, 8, 128), F32),
     }
     sems = {
         "x_sem": (nz,), "c_sem": (2,), "w_sem": (2,), "b_sem": None, "m_sem": (4,),
         "z_recv": (nz,), "mid_recv": (nz,), "last_recv": (nz,), "core_recv": (nz,),
         "ring_recv": (2, 2, nz // 2 + 1), "wy_recv": None, "ay_recv": None, "az_recv": None,
-        "dz_recv": None, "dy_recv": None, "ss_recv": None, "send": (11,),
+        "dz_recv": None, "dy_recv": None, "ss_recv": None,
+        "gp_recv": (nz,), "pm_recv": None, "mn_recv": None, "dd_recv": None, "send": (15,),
     }
     held = {
         "up": ((2, nz, rows, cols), F32),
         "wb": ((2, nz, ny, 64, cols), BF16),
         "wf": ((2, 64, cols), F32),
         "mn": ((4, 8, cols), F32),
-        "factor": ((8, 128), F32),
+        "factor": ((2, 8, 128), F32),
     }
     names = tuple(vmem) + tuple(sems)
     dma = pltpu.SemaphoreType.DMA
@@ -68,9 +72,10 @@
     x_in, ci_in, cg_in, wi_in, wg_in, bi_in, bg_in, fi_in, si_in, fg_in, sg_in = (r[n] for n in ARGS)
     up, wb, wf, mn, factor = (r[n] for n in HELD)
     (
-        xb, cb, ct, gh, gl, st, bb, mo, sb, ry, tz, rz, db, dd, gm, gb, ss,
+        xb, cb, ct, gg, gp, st, bb, mo, sb, ry, tz, rz, db, dd, gm, gb, pm, pn, dp, ss,
         x_sem, c_sem, w_sem, b_sem, m_sem, z_recv, mid_recv, last_recv, core_recv,
-        ring_recv, wy_recv, ay_recv, az_recv, dz_recv, dy_recv, ss_recv, send,
+        ring_recv, wy_recv, ay_recv, az_recv, dz_recv, dy_recv, ss_recv,
+        gp_recv, pm_recv, mn_recv, dd_recv, send,
     ) = (r[n] for n in names)
     slab, rows, rank = 64 // nx, ny * 64, st.shape[2]
     z, y = lax.axis_index("fs_0"), lax.axis_index("fs_1")
@@ -173,12 +178,16 @@
         drain(bb.at[c, zz_of(k), own_l, pl.ds(0, nx - 1)], mid_recv.at[k])
         last_sends(k)
 
+    partner = {"tp_1": 1 - c}
     own = bb.at[c, z, own_l, own_m]
     for k in range(nz - 1, 0, -1):
         sign, half = 2 * (k % 2) - 1, (k + 1) // 2
         at_peer = nz - 1 if k == nz - 1 else (k + 1 if k % 2 else k - 1)
         push(own, own, 0, z_recv.at[at_peer], peer_z((sign * half) % nz))
     mid_sends(0)
+    for i in range(4):
+        drain(mo.at[i], m_sem.at[i])
+    push(mo.at[pl.ds(2 * (1 - c), 2)], pm, 12, pm_recv, partner)
     for d in far_first(ny):
         push(wb.at[:, z, y], wb.at[:, z, y], 3, wy_recv, peer_y(d))
 
@@ -187,8 +196,9 @@
         for p in range(2):
             g = jnp.dot(ct[p], xb[k], preferred_element_type=F32)
             hi = g.astype(BF16)
-            gh[k, p] = hi
-            gl[k, p] = (g - hi.astype(F32)).astype(BF16)
+            gg[k, p, 0] = hi
+            gg[k, p, 1] = (g - hi.astype(F32)).astype(BF16)
+        push(gg.at[k, 1 - c], gp.at[k], 11, gp_recv.at[k], partner)
         return 0
 
     def each(first, last, duty):
@@ -235,30 +245,28 @@
         b = bb[1, j]
         return jnp.concatenate([b[l, m] for m in range(ny) for l in range(nx)], axis=0)
 
-    def core_send(k):
+    def own_basis(j):
+        blocks = []
+        for yy in range(ny):
+            for xx in range(nx):
+                blocks.append(bb[c, j, yy * (1 - c) + xx * c, xx * (1 - c) + yy * c])
+        return jnp.concatenate(blocks, axis=0)
+
+    st[...] = jnp.zeros_like(st)
+
+    def small_step(k, _):
         zz = zz_of(k)
         drain(bb.at[c, zz, pl.ds(0, ny - 1)], last_recv.at[k])
-        push(bb.at[c, zz], bb.at[c, zz], 5, core_recv.at[k], {"tp_1": 1 - c})
-
-    def small_step(k):
-        zz = zz_of(k)
-        drain(bb.at[1 - c, zz], core_recv.at[k])
-        for p in range(2):
-            b = basis(p, zz)
-            st[p] += jnp.dot(gh[k, p], b, preferred_element_type=F32) + jnp.dot(
-                gl[k, p], b, preferred_element_type=F32
+        push(bb.at[c, zz], bb.at[c, zz], 5, core_recv.at[k], partner)
+        drain(gp.at[k], gp_recv.at[k])
+        b = own_basis(zz)
+        for h, part in ((0, gg.at[k, c]), (1, gp.at[k])):
+            st[h] += jnp.dot(part[0], b, preferred_element_type=F32) + jnp.dot(
+                part[1], b, preferred_element_type=F32
             )
-
-    st[...] = jnp.zeros_like(st)
-    core_send(0)
-
-    def body(k, _):
-        core_send(k + 1)
-        small_step(k)
         return 0
 
-    lax.fori_loop(0, nz - 1, body, 0)
-    small_step(nz - 1)
+    lax.fori_loop(0, nz, small_step, 0)
 
     parts = [st[p].T.reshape(rank // 8, 8, st.shape[1]) for p in range(2)]
     sb[...] = jnp.concatenate(parts, axis=1).astype(BF16).reshape(sb.shape)
@@ -272,17 +280,15 @@
     gm[...] = jnp.zeros_like(gm)
 
     def gram_step(j, _):
-        for p in range(2):
-            b = bb[p, j].reshape(rows, rank)
-            gm[p] += lax.dot_general(b, b, (((0,), (0,)), ((), ())), preferred_element_type=F32)
+        b = bb[c, j].reshape(rows, rank)
+        gm[...] += lax.dot_general(b, b, (((0,), (0,)), ((), ())), preferred_element_type=F32)
         return 0
 
     lax.fori_loop(0, nz, gram_step, 0)
-    for p in range(2):
-        gram = gm[p]
-        hi = gram.astype(BF16)
-        gb[p, 0] = hi
-        gb[p, 1] = (gram - hi.astype(F32)).astype(BF16)
+    gram = gm[...]
+    hi = gram.astype(BF16)
+    gb[0] = hi
+    gb[1] = (gram - hi.astype(F32)).astype(BF16)
     drain(ry, ay_recv)
     total = sb[:, y].astype(F32)
     for d in range(1, ny):
@@ -295,17 +301,17 @@
     for d in range(1, nz):
         small += rz[d - 1].astype(F32)
 
-    for i in range(4):
-        drain(mo.at[i], m_sem.at[i])
-    first = jnp.concatenate([mo[0], mo[2]], axis=0)
-    second = jnp.concatenate([mo[1], mo[3]], axis=0)
+    drain(pm, pm_recv)
+    first = jnp.concatenate([mo[2 * c], pm[0]], axis=0)
+    second = jnp.concatenate([mo[2 * c + 1], pm[1]], axis=0)
     first_new = first_decay * first + (1.0 - first_decay) * small
     second_new = second_decay * second + (1.0 - second_decay) * small * small
     db[z, y] = (first_new / (jnp.sqrt(second_new) + 1e-08)).astype(BF16)
     for d in far_first(nz):
         push(db.at[z, y], db.at[z, y], 8, dz_recv, peer_z(d))
-    mn[0], mn[1] = first_new[:8], second_new[:8]
-    mn[2], mn[3] = first_new[8:], second_new[8:]
+    mn[2 * c], mn[2 * c + 1] = first_new[:8], second_new[:8]
+    pn[0], pn[1] = first_new[8:], second_new[8:]
+    push(pn, mn.at[pl.ds(2 * c, 2)], 13, mn_recv, partner)
     if nz > 2:
         ring_wait(2)
         for s in (3,):
@@ -320,21 +326,26 @@
     drain(db.at[:, pl.ds(0, ny - 1)], dy_recv)
 
     directions = db[...].reshape(nz * ny, 16, db.shape[3]).astype(F32)
-    sums = []
-    for p in range(2):
-        d32 = directions[:, 8 * p : 8 * p + 8].reshape(rank, -1)
-        dd[p] = d32.astype(BF16)
-        q = jnp.dot(gb[p, 0], dd[p], preferred_element_type=F32)
-        q += jnp.dot(gb[p, 1], dd[p], preferred_element_type=F32)
-        sums.append(jnp.maximum(jnp.sum(q * d32), 0.0))
-    row = lax.broadcasted_iota(jnp.int32, (8, 128), 0)
-    ss[me_tp] = jnp.where(row == 0, sums[0], sums[1])
+    d_own, d_other = (directions[:, 8 * h : 8 * h + 8].reshape(rank, -1) for h in range(2))
+    dd[c] = d_own.astype(BF16)
+    dp[...] = d_other.astype(BF16)
+    push(dp, dd.at[c], 14, dd_recv, partner)
+    total = jnp.zeros((rank, db.shape[3]), F32)
+    for d32, dh in ((d_own, dd[c]), (d_other, dp[...])):
+        q = jnp.dot(gb[0], dh, preferred_element_type=F32)
+        q += jnp.dot(gb[1], dh, preferred_element_type=F32)
+        total += q * d32
+    ss[me_tp] = jnp.full((8, 128), jnp.maximum(jnp.sum(total), 0.0), F32)
     mine = ss.at[me_tp]
     for d in far_first(nx):
         for cc in (0, 1):
             push(mine, mine, 10, ss_recv, {"tp_0": lax.rem(x + d, nx), "tp_1": cc})
     push(mine, mine, 10, ss_recv, {"tp_1": 1 - c})
 
+    for k in range(nz):
+        drain(bb.at[1 - c, zz_of(k)], core_recv.at[k])
+    drain(dd.at[1 - c], dd_recv)
+
     def update_step(j, _):
         for p in range(2):
             up[p, j] = jnp.dot(basis(p, j), dd[p], preferred_element_type=F32)
@@ -343,10 +354,12 @@
     lax.fori_loop(0, nz, update_step, 0)
     ring_wait(nz // 2)
     drain(ss.at[pl.ds(0, 2 * nx - 1)], ss_recv)
-    squares = ss[0]
-    for t in range(1, 2 * nx):
-        squares += ss[t]
-    factor[...] = jnp.minimum(1.0, 1.0 / jnp.sqrt(squares / entries + 1e-06))
+    for p in range(2):
+        squares = ss[p]
+        for t in range(1, nx):
+            squares += ss[2 * t + p]
+        factor[p] = jnp.minimum(1.0, 1.0 / jnp.sqrt(squares / entries + 1e-06))
+    drain(mn.at[pl.ds(2 * (1 - c), 2)], mn_recv)
 
     drain(bb.at[c, pl.ds(0, nz - 1), 0, 0], send.at[0])
     drain(bb.at[c, :, pl.ds(0, nx - 1), 0], send.at[1])
@@ -359,13 +372,17 @@
     drain(db.at[pl.ds(0, nz - 1), 0], send.at[8])
     drain(db.at[:, pl.ds(0, ny - 1)], send.at[9])
     drain(ss.at[pl.ds(0, 2 * nx - 1)], send.at[10])
+    drain(gp, send.at[11])
+    drain(pm, send.at[12])
+    drain(pn, send.at[13])
+    drain(dp, send.at[14])
 
 
 def finish_kernel(nz, ny, up, wb, wf, mn, factor, *refs):
     outs, (ob, ck, sem) = refs[:10], refs[10:]
     z, y = lax.axis_index("fs_0"), lax.axis_index("fs_1")
     rows = up.shape[2]
-    factors = (factor[0, 0], factor[1, 0])
+    factors = (factor[0, 0, 0], factor[1, 0, 0])
 
     def put(src, dst, k):
         pltpu.make_async_copy(src, dst, sem.at[k]).start()

time: 55.2 us -> 54.6 us (0.989)
  Pallas kernels: 54.5 us -> 53.8 us
    pallas_call x1, Pallas kernels: 52.9 us -> 52.3 us  [shards(): pl.pallas_call(functools.partial(update_kernel, nz, ny, nx, entries, name...]
where the time goes in v4:
time: 54.6 us; the launch traced here: 54.5 us
  Pallas kernels  53.8 us (99%)
  between operations  0.65 us (1%)
    pallas_call x1, Pallas kernels, shards(): pl.pallas_call(functools.partial(update_kernel, nz, ny, nx, entries, name...  52.3 us
    pallas_call x1, Pallas kernels, shards(): pl.pallas_call(functools.partial(finish_kernel, nz, ny), out_shape=outs,...  1.52 us

profile of v4, /device:TPU:1, one launch (start us, length us, event | category | flops | bytes accessed | tf_op | source)
XLA Modules:
  0.0 54.5 jit_solution(11637408172164194851)
XLA Ops:
  0.6 52.3 %shard_map.186 = (f32[2,8,256,256]{3,2,1,0:T(8,128)S(1)}, bf16[2,8,4,64,256]{4,3,2,1,0:T(8,128)(2,1)S(1)}, f32[2,64,256]{2,1,0:T(8,128)S(1)}, f32[4,8,256]{2,1,0:T(8,128)S(1)}, f32[2,8,128]{2,1,0:T(8,128)S(1)}) custom-call(bf16[2048,2048]{1,0:T(8,128)(2,1)} %refs_0_.1, bf16[2048,256]{1,0:T(8,128)(2,1)} %refs_1_.1, bf16[2048,256]{1,0:T(8,128)(2,1)} %refs_2_.1, ...), custom_call_target="tpu_custom_call" | custom-call | tf_op jit(solution)/shard_map/pallas_call | solution.py:417
  53.0 1.5 %shard_map.187 = (f32[64,256]{1,0:T(8,128)}, f32[64,256]{1,0:T(8,128)}, f32[64,256]{1,0:T(8,128)}, f32[64,256]{1,0:T(8,128)}, f32[8,256]{1,0:T(8,128)}, /*index=...) custom-call(f32[2,8,256,256]{3,2,1,0:T(8,128)S(1)} %get-tuple-elemen, ...), custom_call_target="tpu_custom_call" | custom-call | tf_op jit(solution)/shard_map/pallas_call | solution.py:431

commit v5 on v4

--- a/solution.py
+++ b/solution.py
@@ -208,14 +208,14 @@
 
         lax.fori_loop(first, last, one, 0)
 
-    cut1, cut2 = (nz * 5) // 8, (nz * 6) // 8
+    cut1, cut2, cut3 = max(1, nz // 4), nz // 2, max(1, nz * 3 // 8)
     lax.fori_loop(0, cut1, grad_step, 0)
     each(1, cut1, z_duty)
     mid_duty(0)
     lax.fori_loop(cut1, cut2, grad_step, 0)
     each(cut1, nz, z_duty)
     lax.fori_loop(cut2, nz, grad_step, 0)
-    each(1, nz, mid_duty)
+    each(1, cut3, mid_duty)
 
     def ring_reach(p, way):
         return nz // 2 if p == way else nz - 1 - nz // 2
@@ -238,6 +238,8 @@
 
     drain(wb.at[:, z, pl.ds(0, ny - 1)], wy_recv)
     ring_send(1)
+    each(cut3, nz, mid_duty)
+
 
     def basis(p, j):
         if p == 0:
@@ -266,16 +268,17 @@
             )
         return 0
 
-    lax.fori_loop(0, nz, small_step, 0)
+    lax.fori_loop(0, nz - 1, small_step, 0)
+    if nz > 2:
+        ring_wait(1)
+        ring_send(2)
+    lax.fori_loop(nz - 1, nz, small_step, 0)
 
     parts = [st[p].T.reshape(rank // 8, 8, st.shape[1]) for p in range(2)]
     sb[...] = jnp.concatenate(parts, axis=1).astype(BF16).reshape(sb.shape)
     for d in far_first(ny):
         yy = lax.rem(y + d, ny)
         push(sb.at[:, yy], ry.at[d - 1], 6, ay_recv, peer_y(d))
-    if nz > 2:
-        ring_wait(1)
-        ring_send(2)
 
     gm[...] = jnp.zeros_like(gm)
 

time: 54.6 us -> 54.1 us (level)
  no operation moved by 1% of the time
where the time goes in v5:
time: 54.1 us; the launch traced here: 54 us
  Pallas kernels  53.3 us (99%)
  between operations  0.65 us (1%)
    pallas_call x1, Pallas kernels, shards(): pl.pallas_call(functools.partial(update_kernel, nz, ny, nx, entries, name...  51.8 us
    pallas_call x1, Pallas kernels, shards(): pl.pallas_call(functools.partial(finish_kernel, nz, ny), out_shape=outs,...  1.52 us

profile of v5, /device:TPU:1, one launch (start us, length us, event | category | flops | bytes accessed | tf_op | source)
XLA Modules:
  0.0 54.0 jit_solution(15812727403655058444)
XLA Ops:
  0.6 51.8 %shard_map.186 = (f32[2,8,256,256]{3,2,1,0:T(8,128)S(1)}, bf16[2,8,4,64,256]{4,3,2,1,0:T(8,128)(2,1)S(1)}, f32[2,64,256]{2,1,0:T(8,128)S(1)}, f32[4,8,256]{2,1,0:T(8,128)S(1)}, f32[2,8,128]{2,1,0:T(8,128)S(1)}) custom-call(bf16[2048,2048]{1,0:T(8,128)(2,1)} %refs_0_.1, bf16[2048,256]{1,0:T(8,128)(2,1)} %refs_1_.1, bf16[2048,256]{1,0:T(8,128)(2,1)} %refs_2_.1, ...), custom_call_target="tpu_custom_call" | custom-call | tf_op jit(solution)/shard_map/pallas_call | solution.py:420
  52.5 1.5 %shard_map.187 = (f32[64,256]{1,0:T(8,128)}, f32[64,256]{1,0:T(8,128)}, f32[64,256]{1,0:T(8,128)}, f32[64,256]{1,0:T(8,128)}, f32[8,256]{1,0:T(8,128)}, /*index=...) custom-call(f32[2,8,256,256]{3,2,1,0:T(8,128)S(1)} %get-tuple-elemen, ...), custom_call_target="tpu_custom_call" | custom-call | tf_op jit(solution)/shard_map/pallas_call | solution.py:434

commit v6 on v5

--- a/solution.py
+++ b/solution.py
@@ -51,7 +51,7 @@
         "x_sem": (nz,), "c_sem": (2,), "w_sem": (2,), "b_sem": None, "m_sem": (4,),
         "z_recv": (nz,), "mid_recv": (nz,), "last_recv": (nz,), "core_recv": (nz,),
         "ring_recv": (2, 2, nz // 2 + 1), "wy_recv": None, "ay_recv": None, "az_recv": None,
-        "dz_recv": None, "dy_recv": None, "ss_recv": None,
+        "dz_recv": (nz,), "dy_recv": None, "ss_recv": None,
         "gp_recv": (nz,), "pm_recv": None, "mn_recv": None, "dd_recv": None, "send": (15,),
     }
     held = {
@@ -87,6 +87,12 @@
     def far_first(n):
         return sorted(range(1, n), key=lambda d: -min(d, n - d))
 
+    def far_offset(k):
+        return ((2 * (k % 2) - 1) * ((k + 1) // 2)) % nz
+
+    def far_index(k):
+        return nz - 1 if k == nz - 1 else (k + 1 if k % 2 else k - 1)
+
     def zz_of(k):
         sign = 2 * lax.rem(k, 2) - 1 if not isinstance(k, int) else 2 * (k % 2) - 1
         return lax.rem(z + sign * ((k + 1) // 2) + nz, nz)
@@ -181,9 +187,7 @@
     partner = {"tp_1": 1 - c}
     own = bb.at[c, z, own_l, own_m]
     for k in range(nz - 1, 0, -1):
-        sign, half = 2 * (k % 2) - 1, (k + 1) // 2
-        at_peer = nz - 1 if k == nz - 1 else (k + 1 if k % 2 else k - 1)
-        push(own, own, 0, z_recv.at[at_peer], peer_z((sign * half) % nz))
+        push(own, own, 0, z_recv.at[far_index(k)], peer_z(far_offset(k)))
     mid_sends(0)
     for i in range(4):
         drain(mo.at[i], m_sem.at[i])
@@ -293,12 +297,14 @@
     gb[0] = hi
     gb[1] = (gram - hi.astype(F32)).astype(BF16)
     drain(ry, ay_recv)
-    total = sb[:, y].astype(F32)
-    for d in range(1, ny):
-        total += ry[d - 1].astype(F32)
-    tz[...] = total.astype(BF16)
-    for d in far_first(nz):
-        push(tz.at[lax.rem(z + d, nz)], rz.at[d - 1], 7, az_recv, peer_z(d))
+    for d in far_first(nz) + [0]:
+        zz = lax.rem(z + d, nz)
+        total = sb[zz, y].astype(F32)
+        for e in range(1, ny):
+            total += ry[e - 1, zz].astype(F32)
+        tz[zz] = total.astype(BF16)
+        if d:
+            push(tz.at[zz], rz.at[d - 1], 7, az_recv, peer_z(d))
     drain(rz, az_recv)
     small = tz[z].astype(F32)
     for d in range(1, nz):
@@ -310,8 +316,19 @@
     first_new = first_decay * first + (1.0 - first_decay) * small
     second_new = second_decay * second + (1.0 - second_decay) * small * small
     db[z, y] = (first_new / (jnp.sqrt(second_new) + 1e-08)).astype(BF16)
-    for d in far_first(nz):
-        push(db.at[z, y], db.at[z, y], 8, dz_recv, peer_z(d))
+    for k in range(nz - 1, 0, -1):
+        push(db.at[z, y], db.at[z, y], 8, dz_recv.at[far_index(k)], peer_z(far_offset(k)))
+
+    def direction_sends(k):
+        block = db.at[zz_of(k), y]
+        for d in far_first(ny):
+            push(block, block, 9, dy_recv, peer_y(d))
+
+    def direction_duty(k):
+        drain(db.at[zz_of(k), y], dz_recv.at[k])
+        direction_sends(k)
+
+    direction_sends(0)
     mn[2 * c], mn[2 * c + 1] = first_new[:8], second_new[:8]
     pn[0], pn[1] = first_new[8:], second_new[8:]
     push(pn, mn.at[pl.ds(2 * c, 2)], 13, mn_recv, partner)
@@ -320,9 +337,7 @@
         for s in (3,):
             if s <= nz // 2:
                 ring_send(s)
-    drain(db.at[pl.ds(0, nz - 1), y], dz_recv)
-    for d in far_first(ny):
-        push(db.at[:, y], db.at[:, y], 9, dy_recv, peer_y(d))
+    each(1, nz, direction_duty)
     if nz > 4:
         ring_wait(3)
         ring_send(4)

time: 54.1 us -> 53.3 us (0.985)
  Pallas kernels: 53.3 us -> 52.6 us
    pallas_call x1, Pallas kernels: 51.8 us -> 51.1 us  [shards(): pl.pallas_call(functools.partial(update_kernel, nz, ny, nx, entries, name...]
where the time goes in v6:
time: 53.3 us
  Pallas kernels  52.6 us (99%)
  between operations  0.65 us (1%)
    pallas_call x1, Pallas kernels, shards(): pl.pallas_call(functools.partial(update_kernel, nz, ny, nx, entries, name...  51.1 us
    pallas_call x1, Pallas kernels, shards(): pl.pallas_call(functools.partial(finish_kernel, nz, ny), out_shape=outs,...  1.52 us

profile of v6, /device:TPU:1, one launch (start us, length us, event | category | flops | bytes accessed | tf_op | source)
XLA Modules:
  0.0 53.3 jit_solution(1511814394731822328)
XLA Ops:
  0.6 51.1 %shard_map.186 = (f32[2,8,256,256]{3,2,1,0:T(8,128)S(1)}, bf16[2,8,4,64,256]{4,3,2,1,0:T(8,128)(2,1)S(1)}, f32[2,64,256]{2,1,0:T(8,128)S(1)}, f32[4,8,256]{2,1,0:T(8,128)S(1)}, f32[2,8,128]{2,1,0:T(8,128)S(1)}) custom-call(bf16[2048,2048]{1,0:T(8,128)(2,1)} %refs_0_.1, bf16[2048,256]{1,0:T(8,128)(2,1)} %refs_1_.1, bf16[2048,256]{1,0:T(8,128)(2,1)} %refs_2_.1, ...), custom_call_target="tpu_custom_call" | custom-call | tf_op jit(solution)/shard_map/pallas_call | solution.py:435
  51.7 1.5 %shard_map.187 = (f32[64,256]{1,0:T(8,128)}, f32[64,256]{1,0:T(8,128)}, f32[64,256]{1,0:T(8,128)}, f32[64,256]{1,0:T(8,128)}, f32[8,256]{1,0:T(8,128)}, /*index=...) custom-call(f32[2,8,256,256]{3,2,1,0:T(8,128)S(1)} %get-tuple-elemen, ...), custom_call_target="tpu_custom_call" | custom-call | tf_op jit(solution)/shard_map/pallas_call | solution.py:449
